TPU v7x, 32 devices: a whole 2x2x4 slice. The times are simulated.
32 devices in a mesh: ep: 8 (over z, x), tp: 4 (over y, core).
Axes of the slice: x: 2, y: 2, z: 4, core: 2. Of those that a mesh axis runs over, the one named last changes fastest.
Arguments:
- mixer_input: bfloat16 [4096, 2048], P(('ep', 'tp')), may hold values from -6 to 6
- log_decay: float32 [4096, 8], P('ep', 'tp'), may hold values from -0.8 to 0
- mixer_gain: float32 [2048], replicated, may hold values from 0.1 to 1.9
- query_weight: bfloat16 [2048, 1024], P(None, 'tp'), may hold values from -0.125 to 0.125
- key_weight: bfloat16 [2048, 1024], P(None, 'tp'), may hold values from -0.125 to 0.125
- value_weight: bfloat16 [2048, 2048], P(None, 'tp'), may hold values from -0.125 to 0.125
- gate_weight: bfloat16 [2048, 2048], P(None, 'tp'), may hold values from -0.125 to 0.125
- head_gain: float32 [2048], P('tp'), may hold values from 0.1 to 1.9
- output_weight: bfloat16 [2048, 2048], P('tp'), may hold values from -0.125 to 0.125
- expert_input: bfloat16 [4096, 2048], P(('ep', 'tp')), may hold values from -6 to 6
- expert_gain: float32 [2048], replicated, may hold values from 0.1 to 1.9
- routes: int32 [4096, 2], P(('ep', 'tp')), may hold values from 0 to 31, as said below
- group_weight: float32 [4096], P(('ep', 'tp')), may hold values from 0.3 to 1
- pair_weight: float32 [4096, 2], P(('ep', 'tp')), may hold values from 0.2 to 1
- expert_gate: bfloat16 [32, 2048, 1024], P(('ep', 'tp')), may hold values from -0.125 to 0.125
- expert_up: bfloat16 [32, 2048, 1024], P(('ep', 'tp')), may hold values from -0.125 to 0.125
- expert_down: bfloat16 [32, 1024, 2048], P(('ep', 'tp')), may hold values from -0.1875 to 0.1875
Outputs:
- mixer_output: bfloat16 [4096, 2048], P(('ep', 'tp'))
- expert_output: bfloat16 [4096, 2048], P(('ep', 'tp'))
Inputs may be any that keep to these rules, and one draw needn't show every extreme that they name: `routes`: in the rows of one device each expert is named at most 12 times; one expert is named exactly 12 times in the rows of every device. A row names two different experts of the same group, a group being 8 consecutive expert numbers.
All inputs are finite; a program needn't handle non-finite values.
Results may differ from a plain program's by a relative error of at most 0.023.
Values may be sent and summed in bfloat16 or wider, within the bound.
A program may use at most 128 MiB of HBM per device.

v0:
```python
import functools
import math

import jax
import jax.numpy as jnp
import numpy as np
from jax import lax
from jax.experimental import pallas as pl
from jax.experimental.pallas import tpu as pltpu
from jax.sharding import PartitionSpec as P

KEY_DIM = 128
VALUE_DIM = 256
TOPK = 2
GROUPS = 4
LANES = 128
EPSILON = 1e-05
THETA = 10000.0
CHUNKS = 4
LOW = 64
MESH = pl.DeviceIdType.MESH
F32 = jnp.float32
BF16 = jnp.bfloat16


def ceil_to(value, unit):
    return -(-value // unit) * unit


def xor(index, mask):
    out = index
    bit = 1
    while bit <= mask:
        if mask & bit:
            out = out + bit * (1 - 2 * ((index // bit) % 2))
        bit *= 2
    return out


def dot(a, b):
    return jnp.dot(a, b, preferred_element_type=F32)


def rope_tables(length):
    half = KEY_DIM // 2
    frequency = THETA ** (-np.arange(half, dtype=np.float64) / half)
    frequency = np.concatenate([frequency, frequency])
    fine = np.arange(LOW)[:, None] * frequency
    coarse = (np.arange(length // LOW) * LOW)[:, None] * frequency
    return (
        np.stack([np.cos(coarse), np.sin(coarse)], axis=1).astype(np.float32),
        np.stack([np.cos(fine), np.sin(fine)], axis=0).astype(np.float32),
    )


def norm_rows(source, gain, store, rows, step=32):
    @pl.loop(0, rows // step)
    def _(i):
        at = pl.ds(pl.multiple_of(i * step, step), step)
        x = source[at, :].astype(F32)
        x = x - jnp.mean(x, axis=1, keepdims=True)
        spread = jnp.mean(x * x, axis=1, keepdims=True)
        store(at, (x * lax.rsqrt(spread + EPSILON) * gain[...]).astype(BF16))


def body(sizes, *refs):
    (ep_count, tp_count, cap) = sizes
    (
        xm_hbm, decay, mixer_gain, wq_hbm, wk_hbm, wv_hbm, wg_hbm, head_gain, wo_hbm,
        xe_hbm, expert_gain, routes, group_weight, pair_weight, eg_hbm, eu_hbm, ed_hbm,
        coarse, fine,
        mixer_out, expert_out,
        xm, xe, gathered, w_all, wo, eg, eu, ed, proj, cosine, sine, c_row, c_col,
        choose_t, spread_t, mixing, normed,
        packed, relayed, sent, arrived, acc, hidden, result, returned, combined, final,
        meta_out, meta_in,
        st_out, st_in, tot_out, tot_in, incoming,
        gated, terms, pair_in, far_out, far_in,
        load_sem, one_send, one_recv, z_send, z_recv, p_send, p_recv,
    ) = refs
    ep = lax.axis_index("ep")
    tp = lax.axis_index("tp")
    rows, width = xm.shape
    count = ep_count * tp_count
    plane = count // GROUPS
    cols = width // CHUNKS
    slots = packed.shape[2]
    block = sent.shape[2]
    keyw = wq_hbm.shape[1]
    valw = wv_hbm.shape[1]
    heads = keyw // KEY_DIM
    seg = rows * tp_count
    ff = eg.shape[1]
    me = ep * tp_count + tp
    my_plane = me // plane
    my_place = me % plane
    core = tp % 2
    pairs = tp_count // 2

    def at_flat(flat):
        return (flat // tp_count, flat % tp_count)

    def plane_peer(step):
        return at_flat((my_plane + step) % GROUPS * plane + my_place)

    def place_peer(place):
        return at_flat(my_plane * plane + place)

    strides = [1]
    if ep_count > 2:
        strides.append(2)
    covered = len(strides) if ep_count > 2 else 1
    while covered < ep_count - 1:
        strides.append(covered)
        covered *= 2

    loads = {}

    def load(name, source, target):
        copy = pltpu.make_async_copy(source, target, load_sem.at[len(loads)])
        copy.start()
        loads[name] = copy

    load("xm", xm_hbm, xm)
    load("xe", xe_hbm, xe)

    barrier = pltpu.get_barrier_semaphore()
    greeted = 0
    for step in range(1, GROUPS):
        pl.semaphore_signal(barrier, inc=1, device_id=plane_peer(step), device_id_type=MESH)
        greeted += 1
    for mask in range(1, plane):
        pl.semaphore_signal(
            barrier, inc=1, device_id=place_peer(xor(my_place, mask)), device_id_type=MESH
        )
        greeted += 1
    for stride in sorted(set(strides)):
        for other in ((ep + stride) % ep_count, (ep + ep_count - stride) % ep_count):
            pl.semaphore_signal(barrier, inc=1, device_id=(other, tp), device_id_type=MESH)
            greeted += 1

    loads["xm"].wait()
    load("wk", wk_hbm, w_all.at[:, pl.ds(0, keyw)])
    load("wv", wv_hbm, w_all.at[:, pl.ds(keyw, valw)])
    load("wq", wq_hbm, w_all.at[:, pl.ds(keyw + valw, keyw)])
    load("wg", wg_hbm, w_all.at[:, pl.ds(2 * keyw + valw, valw)])
    load("eg", eg_hbm.at[0], eg)
    load("eu", eu_hbm.at[0], eu)
    load("ed", ed_hbm.at[0], ed)
    load("wo", wo_hbm, wo)

    singles = []

    def send(source, target, device, when=None):
        index = len(singles)
        copy = pltpu.make_async_remote_copy(
            src_ref=source, dst_ref=target, send_sem=one_send.at[index],
            recv_sem=one_recv.at[index], device_id=device, device_id_type=MESH,
        )
        singles.append((copy, when))
        if when is None:
            copy.start()
        else:
            pl.when(when)(copy.start)
        return copy

    def keep_mixer(at, value):
        gathered[tp, at, :] = value

    norm_rows(xm, mixer_gain, keep_mixer, rows)
    pl.semaphore_wait(barrier, greeted)
    own = gathered.at[tp]
    far_arrivals = [
        send(own, own, {"tp": xor(tp, far)}) for far in range(2, tp_count, 2)
    ]
    near_arrival = send(own, own, {"tp": xor(tp, 1)})

    loads["xe"].wait()

    def keep_expert(at, value):
        normed[at, :] = value

    norm_rows(xe, expert_gain, keep_expert, rows)

    sub = lax.broadcasted_iota(jnp.int32, (rows, rows), 0)
    lane = lax.broadcasted_iota(jnp.int32, (rows, rows), 1)

    def stacked(lines):
        out = jnp.zeros((rows, rows), F32)
        for i, line in enumerate(lines):
            out = jnp.where(sub == i, line, out)
        return jnp.transpose(out)

    route = routes[...].astype(F32)
    picks = [route[k : k + 1, :] for k in range(TOPK)]
    columns = stacked(picks)
    pick_cols = [columns[:, k : k + 1] for k in range(TOPK)]
    earlier = sub < lane
    group = jnp.floor((picks[0] + 0.5) / plane)
    group_col = jnp.floor((pick_cols[0] + 0.5) / plane)

    def tally(hits):
        return jnp.sum(jnp.where(hits & earlier, 1.0, 0.0), axis=0, keepdims=True)

    place = group * slots + tally(group_col == group)
    lines = []
    for k in range(TOPK):
        hits = pick_cols[0] == picks[k]
        for other in range(1, TOPK):
            hits = hits | (pick_cols[other] == picks[k])
        lines.append((picks[k] - group * plane) * cap + tally(hits) + 1.0)
        lines.append(group_weight[...] * pair_weight[k : k + 1, :])
    lines.append(place)
    columns = stacked(lines)
    n_slots = GROUPS * slots
    choose = jnp.where(
        lax.broadcasted_iota(jnp.int32, (n_slots, rows), 0).astype(F32) == place, 1.0, 0.0
    ).astype(BF16)
    place_col = columns[:, 2 * TOPK : 2 * TOPK + 1]
    choose_t[...] = jnp.where(
        lax.broadcasted_iota(jnp.int32, (rows, n_slots), 1).astype(F32) == place_col, 1.0, 0.0
    ).astype(BF16)
    details = dot(choose, columns.astype(BF16)).astype(BF16)
    meta_out[...] = details.reshape(meta_out.shape)
    meta_in[my_plane] = meta_out[my_plane]
    steps = [2, 1, 3] if GROUPS == 4 else list(range(1, GROUPS))
    meta_arrivals = [
        send(
            meta_out.at[(my_plane + step) % GROUPS], meta_in.at[my_plane], plane_peer(step)
        )
        for step in steps
    ]

    def z_copies(phase, c, source, target):
        target[c, my_plane] = source[c, my_plane]
        for step in steps:
            pltpu.make_async_remote_copy(
                src_ref=source.at[c, (my_plane + step) % GROUPS],
                dst_ref=target.at[c, my_plane],
                send_sem=z_send.at[phase, c],
                recv_sem=z_recv.at[phase, c],
                device_id=plane_peer(step),
                device_id_type=MESH,
            ).start()

    def p_copies(phase, c, source, target):
        target[c, my_place] = source[c, my_place]
        for mask in range(plane - 1, 0, -1):
            other = xor(my_place, mask)
            pltpu.make_async_remote_copy(
                src_ref=source.at[c, other],
                dst_ref=target.at[c, my_place],
                send_sem=p_send.at[phase, c],
                recv_sem=p_recv.at[phase, c],
                device_id=place_peer(other),
                device_id_type=MESH,
            ).start()

    def wait_all(buffer, c, blocks, sem):
        part = buffer.at[c, pl.ds(0, blocks)]
        pltpu.make_async_copy(part, part, sem).wait()

    for c in range(CHUNKS):
        value = dot(choose, normed[:, c * cols : (c + 1) * cols]).astype(BF16)
        packed[c] = value.reshape(packed.shape[1:])
        z_copies(0, c, packed, relayed)

    sign = jnp.where(lax.broadcasted_iota(jnp.int32, (LOW, KEY_DIM), 1) < KEY_DIM // 2, -1.0, 1.0)

    @pl.loop(0, seg // LOW)
    def _(i):
        pair = coarse[ep * (seg // LOW) + i]
        at = pl.ds(pl.multiple_of(i * LOW, LOW), LOW)
        cosine[at, :] = pair[0:1] * fine[0] - pair[1:2] * fine[1]
        sine[at, :] = (pair[1:2] * fine[0] + pair[0:1] * fine[1]) * sign

    running = jnp.concatenate([decay[...], jnp.zeros((8 - heads, seg), F32)], axis=0)
    along = lax.broadcasted_iota(jnp.int32, running.shape, 1)
    shift = 1
    while shift < seg:
        running = running + jnp.where(along >= shift, pltpu.roll(running, shift, 1), 0.0)
        shift *= 2
    c_row[...] = running
    c_col[...] = jnp.transpose(running)

    for name in ("wk", "wv", "wq", "wg"):
        loads[name].wait()
    n_out = 2 * keyw + 2 * valw
    tile = 256 if n_out % 256 == 0 else 128

    def project(pair):
        at = pl.ds(pl.multiple_of(pair * 2 * rows, 2 * rows), 2 * rows)

        @pl.loop(0, n_out // tile)
        def _(n):
            part = pl.ds(pl.multiple_of(n * tile, tile), tile)
            lhs = gathered[pl.ds(pair * 2, 2)].reshape(2 * rows, width)
            proj[at, part] = dot(lhs, w_all[:, part]).astype(BF16)

    near_arrival.wait_recv()
    my_pair = tp // 2
    project(my_pair)

    for copy in meta_arrivals:
        copy.wait_recv()
    info = meta_in[...].reshape(n_slots, LANES).astype(F32)
    source = lax.broadcasted_iota(jnp.int32, (n_slots, 1), 0).astype(F32)
    source = jnp.floor((source + 0.5) / slots)
    n_pos = plane * block
    position = lax.broadcasted_iota(jnp.int32, (n_slots, n_pos), 1).astype(F32)
    spread = jnp.zeros((n_slots, n_pos), F32)
    shares = jnp.zeros((n_slots, n_pos), F32)
    for k in range(TOPK):
        target = info[:, 2 * k : 2 * k + 1] - 1.0
        expert = jnp.floor((target + 0.5) / cap)
        there = expert * block + source * cap + (target - expert * cap)
        there = jnp.where(target >= 0.0, there, -1.0)
        hit = position == there
        spread = jnp.where(hit, 1.0, spread)
        shares = jnp.where(hit, info[:, 2 * k + 1 : 2 * k + 2], shares)
    mixing[...] = shares.astype(BF16)
    full = ceil_to(n_slots, LANES)
    if full > n_slots:
        spread = jnp.concatenate([spread, jnp.zeros((full - n_slots, n_pos), F32)], axis=0)
    spread_t[...] = jnp.transpose(spread)[:, :n_slots].astype(BF16)

    def relay(c):
        wait_all(relayed, c, GROUPS - 1, z_recv.at[0, c])
        value = dot(spread_t[...], relayed[c].reshape(n_slots, cols)).astype(BF16)
        sent[c] = value.reshape(sent.shape[1:])
        p_copies(0, c, sent, arrived)

    half = CHUNKS // 2
    for c in range(half):
        relay(c)

    passed = []
    for place_in, far in enumerate(range(2, tp_count, 2)):
        far_arrivals[place_in].wait_recv()
        slot = gathered.at[xor(tp, far)]
        passed.append(send(slot, slot, {"tp": xor(tp, 1)}))
    for c in range(half, CHUNKS):
        relay(c)
    for place_in, far in enumerate(range(2, tp_count, 2)):
        passed[place_in].wait_recv()
        project(xor(my_pair, far // 2))

    def rotated(first):
        x = proj[:, first : first + KEY_DIM].astype(F32)
        return x * cosine[...] + pltpu.roll(x, KEY_DIM // 2, 1) * sine[...]

    for h in range(heads):
        key = rotated(h * KEY_DIM).astype(BF16)
        proj[:, h * KEY_DIM : (h + 1) * KEY_DIM] = key
        total = c_row[h : h + 1, seg - 1 : seg]
        remain = jnp.exp(total - c_col[:, h : h + 1])
        weighted = (key.astype(F32) * remain).astype(BF16)
        values = proj[:, keyw + h * VALUE_DIM : keyw + (h + 1) * VALUE_DIM]
        state = lax.dot_general(
            weighted, values, (((0,), (0,)), ((), ())), preferred_element_type=F32
        )
        st_out[0, h * KEY_DIM : (h + 1) * KEY_DIM, :] = state.astype(BF16)
    tot_out[0] = jnp.broadcast_to(c_row[:, seg - 1 : seg], tot_out.shape[1:])

    for i, stride in enumerate(strides):
        @pl.when(ep < stride)
        def _():
            st_in[i] = jnp.zeros(st_in.shape[1:], BF16)
            tot_in[i] = jnp.zeros(tot_in.shape[1:], F32)

    def state_send(slot, i):
        stride = strides[i]
        device = {"ep": (ep + stride) % ep_count}
        goes = ep + stride < ep_count
        return (
            send(tot_out.at[slot], tot_in.at[i], device, goes),
            send(st_out.at[slot], st_in.at[i], device, goes),
        )

    def state_recv(i, copies):
        @pl.when(ep >= strides[i])
        def _():
            for copy in copies:
                copy.wait_recv()

    def state_join(i):
        window = tot_in[0] if i == 1 else incoming_total[0]
        for h in range(heads):
            at = slice(h * KEY_DIM, (h + 1) * KEY_DIM)
            near = st_in[0, at, :].astype(F32) if i == 1 else incoming[at, :]
            scale = jnp.exp(window[h : h + 1, 0:1])
            incoming[at, :] = near + scale * st_in[i, at, :].astype(F32)
        incoming_total[0] = window + tot_in[i]

    incoming_total = [None]
    first_round = [state_send(0, i) for i in range(min(2, len(strides)))]

    loads["eg"].wait()
    loads["eu"].wait()
    ftile = 256

    def gate_up(c):
        wait_all(arrived, c, plane - 1, p_recv.at[0, c])
        deep = slice(c * cols, (c + 1) * cols)

        @pl.loop(0, ff // ftile)
        def _(n):
            part = pl.ds(pl.multiple_of(n * ftile, ftile), ftile)
            upper = pl.ds(pl.multiple_of(ff + n * ftile, ftile), ftile)
            lhs = arrived[c].reshape(n_pos, cols)
            gate = dot(lhs, eg[deep, part])
            up = dot(lhs, eu[deep, part])
            if c > 0:
                gate = gate + acc[:, part]
                up = up + acc[:, upper]
            if c < CHUNKS - 1:
                acc[:, part] = gate
                acc[:, upper] = up
            else:
                hidden[:, part] = (gate / (1.0 + jnp.exp(-gate)) * up).astype(BF16)

    def down(c):
        @pl.loop(0, cols // ftile)
        def _(n):
            part = pl.ds(pl.multiple_of(n * ftile, ftile), ftile)
            wide = pl.ds(pl.multiple_of(c * cols + n * ftile, ftile), ftile)
            value = dot(hidden[...], ed[:, wide]).astype(BF16)
            result[c, :, :, part] = value.reshape(plane, block, ftile)

        p_copies(1, c, result, returned)

    gate_up(0)
    gate_up(1)
    for i, copies in enumerate(first_round):
        state_recv(i, copies)
    if len(strides) > 1:
        state_join(1)
    else:
        incoming[...] = st_in[0].astype(F32)
        incoming_total[0] = tot_in[0]
    later = list(range(2, len(strides)))
    pending = None

    def next_state():
        i = later.pop(0)
        slot = i - 1
        st_out[slot] = incoming[...].astype(BF16)
        tot_out[slot] = incoming_total[0]
        return i, state_send(slot, i)

    def finish_state(waiting):
        i, copies = waiting
        state_recv(i, copies)
        state_join(i)

    if later:
        pending = next_state()
    for c in range(2, CHUNKS):
        gate_up(c)
    loads["ed"].wait()
    if pending:
        finish_state(pending)
        pending = next_state() if later else None
    for c in range(CHUNKS):
        down(c)
    while pending:
        finish_state(pending)
        pending = next_state() if later else None

    loads["wo"].wait()
    for h in range(heads):
        first = keyw + valw + h * KEY_DIM
        proj[:, first : first + KEY_DIM] = rotated(first).astype(BF16)

    def retention(pair):
        base = pair * 2 * rows

        @pl.loop(0, 2)
        def _(b):
            start = pl.multiple_of(base + b * rows, rows)
            at = pl.ds(start, rows)
            t = start + lax.broadcasted_iota(jnp.int32, (rows, seg), 0)
            s = lax.broadcasted_iota(jnp.int32, (rows, seg), 1)
            for h in range(heads):
                first = keyw + valw + h * KEY_DIM
                query = proj[at, first : first + KEY_DIM]
                key = proj[:, h * KEY_DIM : (h + 1) * KEY_DIM]
                values = proj[:, keyw + h * VALUE_DIM : keyw + (h + 1) * VALUE_DIM]
                column = c_col[at, h : h + 1]
                gaps = column - c_row[h : h + 1, :]
                weight = jnp.where(t >= s, jnp.exp(jnp.minimum(gaps, 0.0)), 0.0)
                scores = lax.dot_general(
                    query, key, (((1,), (1,)), ((), ())), preferred_element_type=F32
                )
                scaled = (query.astype(F32) * jnp.exp(column)).astype(BF16)
                before = incoming[h * KEY_DIM : (h + 1) * KEY_DIM, :].astype(BF16)
                x = dot((scores * weight).astype(BF16), values) + dot(scaled, before)
                x = x - jnp.mean(x, axis=1, keepdims=True)
                spread = jnp.mean(x * x, axis=1, keepdims=True)
                wide = slice(h * VALUE_DIM, (h + 1) * VALUE_DIM)
                x = x * lax.rsqrt(spread + EPSILON) * head_gain[:, wide]
                first = 2 * keyw + valw + h * VALUE_DIM
                gate = proj[at, first : first + VALUE_DIM].astype(F32)
                gated[at, wide] = (gate / (1.0 + jnp.exp(-gate)) * x).astype(BF16)

        at = pl.ds(pl.multiple_of(base, 2 * rows), 2 * rows)

        @pl.loop(0, width // ftile)
        def _(n):
            part = pl.ds(pl.multiple_of(n * ftile, ftile), ftile)
            value = dot(gated[at, :], wo[:, part]).astype(BF16)
            terms[pl.ds(pair * 2, 2), :, part] = value.reshape(2, rows, ftile)

    def add_rows(store, parts):
        @pl.loop(0, rows // 32)
        def _(i):
            at = pl.ds(pl.multiple_of(i * 32, 32), 32)
            total = parts[0](at).astype(F32)
            for part in parts[1:]:
                total = total + part(at).astype(F32)
            store(at, total.astype(BF16))

    def reduce_pair(i):
        pair = xor(my_pair, i)
        retention(pair)
        return send(terms.at[pair * 2 + 1 - core], pair_in.at[i], {"tp": xor(tp, 1)})

    from_core = {i: reduce_pair(i) for i in range(1, pairs)}
    from_far = []
    for i in range(1, pairs):
        from_core[i].wait_recv()
        mine = xor(my_pair, i) * 2 + core

        def keep_far(at, value, i=i):
            far_out[i - 1, at, :] = value

        add_rows(keep_far, [
            lambda at, mine=mine: terms[mine, at, :], lambda at, i=i: pair_in[i, at, :]
        ])
        from_far.append(send(far_out.at[i - 1], far_in.at[i - 1], {"tp": xor(tp, 2 * i)}))
    from_core[0] = reduce_pair(0)

    for c in range(CHUNKS):
        wait_all(returned, c, plane - 1, p_recv.at[1, c])
        value = dot(mixing[...], returned[c].reshape(n_pos, cols)).astype(BF16)
        combined[c] = value.reshape(combined.shape[1:])
        z_copies(1, c, combined, final)
    for c in range(CHUNKS):
        wait_all(final, c, GROUPS - 1, z_recv.at[1, c])
        value = dot(choose_t[...], final[c].reshape(n_slots, cols))
        expert_out[:, c * cols : (c + 1) * cols] = value.astype(BF16)

    from_core[0].wait_recv()
    for copy in from_far:
        copy.wait_recv()

    def keep_out(at, value):
        mixer_out[at, :] = value

    add_rows(keep_out, [
        lambda at: terms[tp, at, :], lambda at: pair_in[0, at, :]
    ] + [lambda at, i=i: far_in[i, at, :] for i in range(pairs - 1)])

    for copy, when in singles:
        if when is None:
            copy.wait_send()
        else:
            pl.when(when)(copy.wait_send)
    for c in range(CHUNKS):
        wait_all(packed, c, GROUPS - 1, z_send.at[0, c])
        wait_all(combined, c, GROUPS - 1, z_send.at[1, c])
        wait_all(sent, c, plane - 1, p_send.at[0, c])
        wait_all(result, c, plane - 1, p_send.at[1, c])


def local(
    ep_count, tp_count,
    mixer_input, log_decay, mixer_gain, query_weight, key_weight, value_weight, gate_weight,
    head_gain, output_weight, expert_input, expert_gain, routes, group_weight, pair_weight,
    expert_gate, expert_up, expert_down,
):
    rows, width = mixer_input.shape
    count = ep_count * tp_count
    plane = count // GROUPS
    cap = 3 * rows * TOPK // (2 * count)
    slots = ceil_to(plane * cap // TOPK, 16)
    block = ceil_to(cap * GROUPS, 16)
    cols = width // CHUNKS
    keyw = query_weight.shape[1]
    valw = value_weight.shape[1]
    heads = keyw // KEY_DIM
    seg = rows * tp_count
    ff = expert_gate.shape[2]
    n_slots = GROUPS * slots
    n_pos = plane * block
    pairs = tp_count // 2
    rounds = max(1, math.ceil(math.log2(ep_count))) + 1
    coarse, fine = rope_tables(seg * ep_count)

    def buf(*shape, dtype=BF16):
        return pltpu.VMEM(shape, dtype)

    dma = pltpu.SemaphoreType.DMA
    scratch = [
        buf(rows, width), buf(rows, width), buf(tp_count, rows, width),
        buf(width, 2 * keyw + 2 * valw), buf(valw, width),
        buf(width, ff), buf(width, ff), buf(ff, width),
        buf(seg, 2 * keyw + 2 * valw),
        buf(seg, KEY_DIM, dtype=F32), buf(seg, KEY_DIM, dtype=F32),
        buf(8, seg, dtype=F32), buf(seg, 8, dtype=F32),
        buf(rows, n_slots), buf(n_pos, n_slots), buf(n_slots, n_pos), buf(rows, width),
        buf(CHUNKS, GROUPS, slots, cols), buf(CHUNKS, GROUPS, slots, cols),
        buf(CHUNKS, plane, block, cols), buf(CHUNKS, plane, block, cols),
        buf(n_pos, 2 * ff, dtype=F32), buf(n_pos, ff),
        buf(CHUNKS, plane, block, cols), buf(CHUNKS, plane, block, cols),
        buf(CHUNKS, GROUPS, slots, cols), buf(CHUNKS, GROUPS, slots, cols),
        buf(GROUPS, slots, LANES), buf(GROUPS, slots, LANES),
        buf(rounds, keyw, VALUE_DIM), buf(rounds, keyw, VALUE_DIM),
        buf(rounds, 8, LANES, dtype=F32), buf(rounds, 8, LANES, dtype=F32),
        buf(keyw, VALUE_DIM, dtype=F32),
        buf(seg, valw), buf(tp_count, rows, width), buf(pairs, rows, width),
        buf(max(1, pairs - 1), rows, width), buf(max(1, pairs - 1), rows, width),
        dma((16,)), dma((32,)), dma((32,)),
        dma((2, CHUNKS)), dma((2, CHUNKS)), dma((2, CHUNKS)), dma((2, CHUNKS)),
    ]
    any_space = pl.BlockSpec(memory_space=pl.ANY)
    vmem = pl.BlockSpec(memory_space=pltpu.VMEM)
    shape = jax.ShapeDtypeStruct((rows, width), BF16)
    return pl.pallas_call(
        functools.partial(body, (ep_count, tp_count, cap)),
        out_shape=(shape, shape),
        in_specs=[
            any_space, vmem, vmem, any_space, any_space, any_space, any_space, vmem, any_space,
            any_space, vmem, vmem, vmem, vmem, any_space, any_space, any_space, vmem, vmem,
        ],
        out_specs=(vmem, vmem),
        scratch_shapes=scratch,
        compiler_params=pltpu.CompilerParams(
            collective_id=0, has_side_effects=True, vmem_limit_bytes=67_000_000
        ),
    )(
        mixer_input, log_decay.T, mixer_gain[None, :], query_weight, key_weight, value_weight,
        gate_weight, head_gain[None, :], output_weight, expert_input, expert_gain[None, :],
        routes.T, group_weight[None, :], pair_weight.T, expert_gate, expert_up, expert_down,
        jnp.asarray(coarse), jnp.asarray(fine),
    )


def solution(mesh):
    return jax.shard_map(
        functools.partial(local, mesh.shape["ep"], mesh.shape["tp"]),
        mesh=mesh,
        in_specs=(
            P(("ep", "tp"), None), P("ep", "tp"), P(), P(None, "tp"), P(None, "tp"),
            P(None, "tp"), P(None, "tp"), P("tp"), P("tp", None), P(("ep", "tp"), None), P(),
            P(("ep", "tp"), None), P(("ep", "tp")), P(("ep", "tp"), None),
            P(("ep", "tp"), None, None), P(("ep", "tp"), None, None),
            P(("ep", "tp"), None, None),
        ),
        out_specs=(P(("ep", "tp"), None), P(("ep", "tp"), None)),
        check_vma=False,
    )
```

profile of v0, /device:TPU:0, one launch (start us, length us, event | category | flops | bytes accessed | tf_op | source)
XLA Modules:
  0.0 80.4 jit_solution(13026441728811215260)
XLA Ops:
  0.6 76.0 %shard_map.194 = (bf16[128,2048]{1,0:T(8,128)(2,1)}, bf16[128,2048]{1,0:T(8,128)(2,1)}) custom-call(bf16[128,2048]{1,0:T(8,128)(2,1)} %refs_0_.1, f32[2,512]{1,0:T(2,128)} %bitcast.9, f32[1,2048]{1,0:T(1,128)} %bitcast.7, bf16[2048,256]{1,0:T(8,128)(2,1)} %refs_3_.1, bf16[2048,256]{1,0:T(8,128)(2,1)} %refs_4_.1, bf16[2048,512]{1,0:T(8,128)(2,1)} %refs_5_.1, ...), custom_call_target="tpu_custom_call" | custom-call | tf_op jit(solution)/shard_map/pallas_call | solution.py:629
  76.6 1.9 %copy.23 = bf16[128,2048]{1,0:T(8,128)(2,1)} copy(bf16[128,2048]{1,0:T(8,128)(2,1)} %get-tuple-element.4) | data formatting | bytes 1048576
  78.5 1.9 %copy.24 = bf16[128,2048]{1,0:T(8,128)(2,1)} copy(bf16[128,2048]{1,0:T(8,128)(2,1)} %get-tuple-element.5) | data formatting | bytes 1048576
where the time goes:
time: 81.8 us; the launch traced here: 80.4 us
  Pallas kernels  76 us (93%)
  local copies, waits for them, and re-layouts  3.76 us (5%)
    pallas_call x1, Pallas kernels, local(): pl.pallas_call(functools.partial(body, (ep_count, tp_count, cap)), out_sh...  76 us
    unnamed x2, local copies, waits for them, and re-layouts  3.76 us

commit v1 on v0

--- a/solution.py
+++ b/solution.py
@@ -1,5 +1,4 @@
 import functools
-import math
 
 import jax
 import jax.numpy as jnp
@@ -16,11 +15,17 @@
 LANES = 128
 EPSILON = 1e-05
 THETA = 10000.0
-CHUNKS = 4
+CHUNKS = 8
+VMEM_LIMIT = 60 * 2**20
+DEEP = (2, 2, 2, 1, 1)
 LOW = 64
 MESH = pl.DeviceIdType.MESH
 F32 = jnp.float32
 BF16 = jnp.bfloat16
+
+ORDER = (
+    ("near_norm",), ("near_project",), ("spread_rows",), ("far_pass",), ("relay", 0), ("relay", 1), ("relay", 2), ("far_norm",), ("relay", 3), ("far_project",), ("states",), ("relay", 4), ("relay", 5), ("gate_up", 0), ("relay", 6), ("gate_up", 1), ("relay", 7), ("gate_up", 2), ("gate_up", 3), ("gate_up", 4), ("state_round", 0), ("down", 0), ("down", 1), ("down", 2), ("down", 3), ("down", 4), ("down", 5), ("down", 6), ("down", 7), ("queries",), ("combine", 0), ("state_round", 1), ("state_rest",), ("far_terms",), ("combine", 1), ("combine", 2), ("far_sums",), ("combine", 3), ("combine", 4), ("near_terms",), ("combine", 5), ("combine", 6), ("combine", 7), ("finish", 0), ("finish", 1), ("finish", 2), ("finish", 3), ("finish", 4), ("finish", 5), ("finish", 6), ("finish", 7), ("mixer_sum",),
+)
 
 
 def ceil_to(value, unit):
@@ -53,6 +58,15 @@
     )
 
 
+def state_strides(ep_count):
+    rounds = []
+    base = 1
+    while base < ep_count:
+        rounds.append([i * base for i in range(1, 4) if i * base < ep_count])
+        base *= 4
+    return rounds
+
+
 def norm_rows(source, gain, store, rows, step=32):
     @pl.loop(0, rows // step)
     def _(i):
@@ -66,21 +80,22 @@
 def body(sizes, *refs):
     (ep_count, tp_count, cap) = sizes
     (
-        xm_hbm, decay, mixer_gain, wq_hbm, wk_hbm, wv_hbm, wg_hbm, head_gain, wo_hbm,
-        xe_hbm, expert_gain, routes, group_weight, pair_weight, eg_hbm, eu_hbm, ed_hbm,
-        coarse, fine,
+        xm_hbm, decay_hbm, mixer_gain_hbm, wq_hbm, wk_hbm, wv_hbm, wg_hbm, head_gain_hbm, wo_hbm,
+        xe_hbm, expert_gain_hbm, routes_hbm, group_weight_hbm, pair_weight_hbm,
+        eg_hbm, eu_hbm, ed_hbm, coarse_hbm, fine_hbm,
         mixer_out, expert_out,
-        xm, xe, gathered, w_all, wo, eg, eu, ed, proj, cosine, sine, c_row, c_col,
+        decay, mixer_gain, head_gain, xe, expert_gain, routes, group_weight, pair_weight,
+        coarse, fine, gathered, mixer_rows, w_all, wo, eg, eu, ed, proj, cosine, sine, c_row, c_col,
         choose_t, spread_t, mixing, normed,
         packed, relayed, sent, arrived, acc, hidden, result, returned, combined, final,
         meta_out, meta_in,
-        st_out, st_in, tot_out, tot_in, incoming,
+        st_out, st_in, tot_out, tot_in, incoming, window_total,
         gated, terms, pair_in, far_out, far_in,
         load_sem, one_send, one_recv, z_send, z_recv, p_send, p_recv,
     ) = refs
     ep = lax.axis_index("ep")
     tp = lax.axis_index("tp")
-    rows, width = xm.shape
+    rows, width = xe.shape
     count = ep_count * tp_count
     plane = count // GROUPS
     cols = width // CHUNKS
@@ -106,13 +121,8 @@
     def place_peer(place):
         return at_flat(my_plane * plane + place)
 
-    strides = [1]
-    if ep_count > 2:
-        strides.append(2)
-    covered = len(strides) if ep_count > 2 else 1
-    while covered < ep_count - 1:
-        strides.append(covered)
-        covered *= 2
+    rounds = state_strides(ep_count)
+    strides = [stride for group in rounds for stride in group]
 
     loads = {}
 
@@ -121,9 +131,19 @@
         copy.start()
         loads[name] = copy
 
-    load("xm", xm_hbm, xm)
     load("xe", xe_hbm, xe)
-
+    load("routes", routes_hbm, routes)
+    load("group_weight", group_weight_hbm, group_weight)
+    load("pair_weight", pair_weight_hbm, pair_weight)
+    load("expert_gain", expert_gain_hbm, expert_gain)
+    small = list(loads)
+    load("xm", xm_hbm, gathered.at[tp])
+    load("mixer_gain", mixer_gain_hbm, mixer_gain)
+    load("decay", decay_hbm, decay)
+    load("head_gain", head_gain_hbm, head_gain)
+    load("coarse", coarse_hbm.at[pl.ds(ep * coarse.shape[0], coarse.shape[0])], coarse)
+    load("fine", fine_hbm, fine)
+    others = [name for name in loads if name not in small]
     barrier = pltpu.get_barrier_semaphore()
     greeted = 0
     for step in range(1, GROUPS):
@@ -139,16 +159,6 @@
             pl.semaphore_signal(barrier, inc=1, device_id=(other, tp), device_id_type=MESH)
             greeted += 1
 
-    loads["xm"].wait()
-    load("wk", wk_hbm, w_all.at[:, pl.ds(0, keyw)])
-    load("wv", wv_hbm, w_all.at[:, pl.ds(keyw, valw)])
-    load("wq", wq_hbm, w_all.at[:, pl.ds(keyw + valw, keyw)])
-    load("wg", wg_hbm, w_all.at[:, pl.ds(2 * keyw + valw, valw)])
-    load("eg", eg_hbm.at[0], eg)
-    load("eu", eu_hbm.at[0], eu)
-    load("ed", ed_hbm.at[0], ed)
-    load("wo", wo_hbm, wo)
-
     singles = []
 
     def send(source, target, device, when=None):
@@ -164,18 +174,23 @@
             pl.when(when)(copy.start)
         return copy
 
-    def keep_mixer(at, value):
-        gathered[tp, at, :] = value
-
-    norm_rows(xm, mixer_gain, keep_mixer, rows)
     pl.semaphore_wait(barrier, greeted)
-    own = gathered.at[tp]
+    slot = gathered.at[tp]
     far_arrivals = [
-        send(own, own, {"tp": xor(tp, far)}) for far in range(2, tp_count, 2)
+        send(xm_hbm, slot, {"tp": xor(tp, far)}) for far in range(2, tp_count, 2)
     ]
-    near_arrival = send(own, own, {"tp": xor(tp, 1)})
-
-    loads["xe"].wait()
+    near_arrival = send(xm_hbm, slot, {"tp": xor(tp, 1)})
+    load("wk", wk_hbm, w_all.at[:, pl.ds(0, keyw)])
+    load("wv", wv_hbm, w_all.at[:, pl.ds(keyw, valw)])
+    load("wq", wq_hbm, w_all.at[:, pl.ds(keyw + valw, keyw)])
+    load("wg", wg_hbm, w_all.at[:, pl.ds(2 * keyw + valw, valw)])
+    load("eg", eg_hbm.at[0], eg)
+    load("eu", eu_hbm.at[0], eu)
+    load("ed", ed_hbm.at[0], ed)
+    load("wo", wo_hbm, wo)
+
+    for name in small:
+        loads[name].wait()
 
     def keep_expert(at, value):
         normed[at, :] = value
@@ -265,11 +280,13 @@
         packed[c] = value.reshape(packed.shape[1:])
         z_copies(0, c, packed, relayed)
 
+    for name in others:
+        loads[name].wait()
     sign = jnp.where(lax.broadcasted_iota(jnp.int32, (LOW, KEY_DIM), 1) < KEY_DIM // 2, -1.0, 1.0)
 
     @pl.loop(0, seg // LOW)
     def _(i):
-        pair = coarse[ep * (seg // LOW) + i]
+        pair = coarse[i]
         at = pl.ds(pl.multiple_of(i * LOW, LOW), LOW)
         cosine[at, :] = pair[0:1] * fine[0] - pair[1:2] * fine[1]
         sine[at, :] = (pair[1:2] * fine[0] + pair[0:1] * fine[1]) * sign
@@ -283,10 +300,12 @@
     c_row[...] = running
     c_col[...] = jnp.transpose(running)
 
-    for name in ("wk", "wv", "wq", "wg"):
-        loads[name].wait()
     n_out = 2 * keyw + 2 * valw
     tile = 256 if n_out % 256 == 0 else 128
+
+    def weights():
+        for name in ("wk", "wv", "wq", "wg"):
+            loads[name].wait()
 
     def project(pair):
         at = pl.ds(pl.multiple_of(pair * 2 * rows, 2 * rows), 2 * rows)
@@ -294,35 +313,52 @@
         @pl.loop(0, n_out // tile)
         def _(n):
             part = pl.ds(pl.multiple_of(n * tile, tile), tile)
-            lhs = gathered[pl.ds(pair * 2, 2)].reshape(2 * rows, width)
+            lhs = mixer_rows[pl.ds(pair * 2, 2)].reshape(2 * rows, width)
             proj[at, part] = dot(lhs, w_all[:, part]).astype(BF16)
 
-    near_arrival.wait_recv()
+    order_of_steps = ORDER
     my_pair = tp // 2
-    project(my_pair)
-
-    for copy in meta_arrivals:
-        copy.wait_recv()
-    info = meta_in[...].reshape(n_slots, LANES).astype(F32)
-    source = lax.broadcasted_iota(jnp.int32, (n_slots, 1), 0).astype(F32)
-    source = jnp.floor((source + 0.5) / slots)
+    far_pairs = range(1, pairs)
     n_pos = plane * block
-    position = lax.broadcasted_iota(jnp.int32, (n_slots, n_pos), 1).astype(F32)
-    spread = jnp.zeros((n_slots, n_pos), F32)
-    shares = jnp.zeros((n_slots, n_pos), F32)
-    for k in range(TOPK):
-        target = info[:, 2 * k : 2 * k + 1] - 1.0
-        expert = jnp.floor((target + 0.5) / cap)
-        there = expert * block + source * cap + (target - expert * cap)
-        there = jnp.where(target >= 0.0, there, -1.0)
-        hit = position == there
-        spread = jnp.where(hit, 1.0, spread)
-        shares = jnp.where(hit, info[:, 2 * k + 1 : 2 * k + 2], shares)
-    mixing[...] = shares.astype(BF16)
-    full = ceil_to(n_slots, LANES)
-    if full > n_slots:
-        spread = jnp.concatenate([spread, jnp.zeros((full - n_slots, n_pos), F32)], axis=0)
-    spread_t[...] = jnp.transpose(spread)[:, :n_slots].astype(BF16)
+    ftile = 256
+
+    def norm_block(place):
+        def keep(at, value):
+            mixer_rows[place, at, :] = value
+
+        norm_rows(gathered.at[place], mixer_gain, keep, rows)
+
+    def near_norm():
+        norm_block(tp)
+        near_arrival.wait_recv()
+        norm_block(xor(tp, 1))
+
+    def near_project():
+        weights()
+        project(my_pair)
+
+    def spread_rows():
+        for copy in meta_arrivals:
+            copy.wait_recv()
+        info = meta_in[...].reshape(n_slots, LANES).astype(F32)
+        source = lax.broadcasted_iota(jnp.int32, (n_slots, 1), 0).astype(F32)
+        source = jnp.floor((source + 0.5) / slots)
+        position = lax.broadcasted_iota(jnp.int32, (n_slots, n_pos), 1).astype(F32)
+        spread = jnp.zeros((n_slots, n_pos), F32)
+        shares = jnp.zeros((n_slots, n_pos), F32)
+        for k in range(TOPK):
+            target = info[:, 2 * k : 2 * k + 1] - 1.0
+            expert = jnp.floor((target + 0.5) / cap)
+            there = expert * block + source * cap + (target - expert * cap)
+            there = jnp.where(target >= 0.0, there, -1.0)
+            hit = position == there
+            spread = jnp.where(hit, 1.0, spread)
+            shares = jnp.where(hit, info[:, 2 * k + 1 : 2 * k + 2], shares)
+        mixing[...] = shares.astype(BF16)
+        full = ceil_to(n_slots, LANES)
+        if full > n_slots:
+            spread = jnp.concatenate([spread, jnp.zeros((full - n_slots, n_pos), F32)], axis=0)
+        spread_t[...] = jnp.transpose(spread)[:, :n_slots].astype(BF16)
 
     def relay(c):
         wait_all(relayed, c, GROUPS - 1, z_recv.at[0, c])
@@ -330,96 +366,122 @@
         sent[c] = value.reshape(sent.shape[1:])
         p_copies(0, c, sent, arrived)
 
-    half = CHUNKS // 2
-    for c in range(half):
-        relay(c)
-
     passed = []
-    for place_in, far in enumerate(range(2, tp_count, 2)):
-        far_arrivals[place_in].wait_recv()
-        slot = gathered.at[xor(tp, far)]
-        passed.append(send(slot, slot, {"tp": xor(tp, 1)}))
-    for c in range(half, CHUNKS):
-        relay(c)
-    for place_in, far in enumerate(range(2, tp_count, 2)):
-        passed[place_in].wait_recv()
-        project(xor(my_pair, far // 2))
+
+    def far_pass():
+        for i in far_pairs:
+            far_arrivals[i - 1].wait_recv()
+            slot = gathered.at[xor(tp, 2 * i)]
+            passed.append(send(slot, slot, {"tp": xor(tp, 1)}))
+
+    def far_norm():
+        for i in far_pairs:
+            norm_block(xor(tp, 2 * i))
+            passed[i - 1].wait_recv()
+            norm_block(xor(tp, 2 * i + 1))
+
+    def far_project():
+        for i in far_pairs:
+            project(xor(my_pair, i))
 
     def rotated(first):
         x = proj[:, first : first + KEY_DIM].astype(F32)
         return x * cosine[...] + pltpu.roll(x, KEY_DIM // 2, 1) * sine[...]
 
-    for h in range(heads):
-        key = rotated(h * KEY_DIM).astype(BF16)
-        proj[:, h * KEY_DIM : (h + 1) * KEY_DIM] = key
-        total = c_row[h : h + 1, seg - 1 : seg]
-        remain = jnp.exp(total - c_col[:, h : h + 1])
-        weighted = (key.astype(F32) * remain).astype(BF16)
-        values = proj[:, keyw + h * VALUE_DIM : keyw + (h + 1) * VALUE_DIM]
-        state = lax.dot_general(
-            weighted, values, (((0,), (0,)), ((), ())), preferred_element_type=F32
-        )
-        st_out[0, h * KEY_DIM : (h + 1) * KEY_DIM, :] = state.astype(BF16)
-    tot_out[0] = jnp.broadcast_to(c_row[:, seg - 1 : seg], tot_out.shape[1:])
-
-    for i, stride in enumerate(strides):
-        @pl.when(ep < stride)
-        def _():
-            st_in[i] = jnp.zeros(st_in.shape[1:], BF16)
-            tot_in[i] = jnp.zeros(tot_in.shape[1:], F32)
-
-    def state_send(slot, i):
-        stride = strides[i]
-        device = {"ep": (ep + stride) % ep_count}
-        goes = ep + stride < ep_count
-        return (
-            send(tot_out.at[slot], tot_in.at[i], device, goes),
-            send(st_out.at[slot], st_in.at[i], device, goes),
-        )
-
-    def state_recv(i, copies):
+    prefix = {}
+
+    def state_send(r):
+        for stride in rounds[r]:
+            i = strides.index(stride)
+            device = {"ep": (ep + stride) % ep_count}
+            goes = ep + stride < ep_count
+            prefix[i] = (
+                send(tot_out.at[r], tot_in.at[i], device, goes),
+                send(st_out.at[r], st_in.at[i], device, goes),
+            )
+
+    def states():
+        for h in range(heads):
+            key = rotated(h * KEY_DIM).astype(BF16)
+            proj[:, h * KEY_DIM : (h + 1) * KEY_DIM] = key
+            total = c_row[h : h + 1, seg - 1 : seg]
+            remain = jnp.exp(total - c_col[:, h : h + 1])
+            weighted = (key.astype(F32) * remain).astype(BF16)
+            values = proj[:, keyw + h * VALUE_DIM : keyw + (h + 1) * VALUE_DIM]
+            state = lax.dot_general(
+                weighted, values, (((0,), (0,)), ((), ())), preferred_element_type=F32
+            )
+            st_out[0, h * KEY_DIM : (h + 1) * KEY_DIM, :] = state.astype(BF16)
+        tot_out[0] = jnp.broadcast_to(c_row[:, seg - 1 : seg], tot_out.shape[1:])
+        for i, stride in enumerate(strides):
+            @pl.when(ep < stride)
+            def _():
+                st_in[i] = jnp.zeros(st_in.shape[1:], BF16)
+                tot_in[i] = jnp.zeros(tot_in.shape[1:], F32)
+        state_send(0)
+
+    def state_recv(i):
         @pl.when(ep >= strides[i])
         def _():
-            for copy in copies:
+            for copy in prefix[i]:
                 copy.wait_recv()
 
-    def state_join(i):
-        window = tot_in[0] if i == 1 else incoming_total[0]
-        for h in range(heads):
-            at = slice(h * KEY_DIM, (h + 1) * KEY_DIM)
-            near = st_in[0, at, :].astype(F32) if i == 1 else incoming[at, :]
-            scale = jnp.exp(window[h : h + 1, 0:1])
-            incoming[at, :] = near + scale * st_in[i, at, :].astype(F32)
-        incoming_total[0] = window + tot_in[i]
-
-    incoming_total = [None]
-    first_round = [state_send(0, i) for i in range(min(2, len(strides)))]
-
-    loads["eg"].wait()
-    loads["eu"].wait()
-    ftile = 256
+    def state_round(r):
+        if r >= len(rounds):
+            return
+        for stride in rounds[r]:
+            i = strides.index(stride)
+            state_recv(i)
+            for h in range(heads):
+                at = slice(h * KEY_DIM, (h + 1) * KEY_DIM)
+                part = st_in[i, at, :].astype(F32)
+                if i > 0:
+                    scale = jnp.exp(window_total[h : h + 1, 0:1])
+                    part = incoming[at, :] + scale * part
+                incoming[at, :] = part
+            window_total[...] = tot_in[i] + (window_total[...] if i > 0 else 0.0)
+        if r + 1 < len(rounds):
+            for h in range(heads):
+                at = slice(h * KEY_DIM, (h + 1) * KEY_DIM)
+                scale = jnp.exp(tot_out[0, h : h + 1, 0:1])
+                whole = st_out[0, at, :].astype(F32) + scale * incoming[at, :]
+                st_out[r + 1, at, :] = whole.astype(BF16)
+            tot_out[r + 1] = tot_out[0] + window_total[...]
+            state_send(r + 1)
+
+    def state_rest():
+        for r in range(2, len(rounds)):
+            state_round(r)
 
     def gate_up(c):
-        wait_all(arrived, c, plane - 1, p_recv.at[0, c])
-        deep = slice(c * cols, (c + 1) * cols)
+        if c == 0:
+            loads["eg"].wait()
+            loads["eu"].wait()
+        group = range(sum(DEEP[:c]), sum(DEEP[: c + 1]))
+        for i in group:
+            wait_all(arrived, i, plane - 1, p_recv.at[0, i])
 
         @pl.loop(0, ff // ftile)
         def _(n):
             part = pl.ds(pl.multiple_of(n * ftile, ftile), ftile)
             upper = pl.ds(pl.multiple_of(ff + n * ftile, ftile), ftile)
-            lhs = arrived[c].reshape(n_pos, cols)
-            gate = dot(lhs, eg[deep, part])
-            up = dot(lhs, eu[deep, part])
-            if c > 0:
-                gate = gate + acc[:, part]
-                up = up + acc[:, upper]
-            if c < CHUNKS - 1:
+            gate = acc[:, part] if c > 0 else 0.0
+            up = acc[:, upper] if c > 0 else 0.0
+            for i in group:
+                lhs = arrived[i].reshape(n_pos, cols)
+                deep = slice(i * cols, (i + 1) * cols)
+                gate = gate + dot(lhs, eg[deep, part])
+                up = up + dot(lhs, eu[deep, part])
+            if c < len(DEEP) - 1:
                 acc[:, part] = gate
                 acc[:, upper] = up
             else:
                 hidden[:, part] = (gate / (1.0 + jnp.exp(-gate)) * up).astype(BF16)
 
     def down(c):
+        if c == 0:
+            loads["ed"].wait()
+
         @pl.loop(0, cols // ftile)
         def _(n):
             part = pl.ds(pl.multiple_of(n * ftile, ftile), ftile)
@@ -429,48 +491,11 @@
 
         p_copies(1, c, result, returned)
 
-    gate_up(0)
-    gate_up(1)
-    for i, copies in enumerate(first_round):
-        state_recv(i, copies)
-    if len(strides) > 1:
-        state_join(1)
-    else:
-        incoming[...] = st_in[0].astype(F32)
-        incoming_total[0] = tot_in[0]
-    later = list(range(2, len(strides)))
-    pending = None
-
-    def next_state():
-        i = later.pop(0)
-        slot = i - 1
-        st_out[slot] = incoming[...].astype(BF16)
-        tot_out[slot] = incoming_total[0]
-        return i, state_send(slot, i)
-
-    def finish_state(waiting):
-        i, copies = waiting
-        state_recv(i, copies)
-        state_join(i)
-
-    if later:
-        pending = next_state()
-    for c in range(2, CHUNKS):
-        gate_up(c)
-    loads["ed"].wait()
-    if pending:
-        finish_state(pending)
-        pending = next_state() if later else None
-    for c in range(CHUNKS):
-        down(c)
-    while pending:
-        finish_state(pending)
-        pending = next_state() if later else None
-
-    loads["wo"].wait()
-    for h in range(heads):
-        first = keyw + valw + h * KEY_DIM
-        proj[:, first : first + KEY_DIM] = rotated(first).astype(BF16)
+    def queries():
+        loads["wo"].wait()
+        for h in range(heads):
+            first = keyw + valw + h * KEY_DIM
+            proj[:, first : first + KEY_DIM] = rotated(first).astype(BF16)
 
     def retention(pair):
         base = pair * 2 * rows
@@ -520,46 +545,60 @@
                 total = total + part(at).astype(F32)
             store(at, total.astype(BF16))
 
+    from_core = {}
+    from_far = []
+
     def reduce_pair(i):
         pair = xor(my_pair, i)
         retention(pair)
-        return send(terms.at[pair * 2 + 1 - core], pair_in.at[i], {"tp": xor(tp, 1)})
-
-    from_core = {i: reduce_pair(i) for i in range(1, pairs)}
-    from_far = []
-    for i in range(1, pairs):
-        from_core[i].wait_recv()
-        mine = xor(my_pair, i) * 2 + core
-
-        def keep_far(at, value, i=i):
-            far_out[i - 1, at, :] = value
-
-        add_rows(keep_far, [
-            lambda at, mine=mine: terms[mine, at, :], lambda at, i=i: pair_in[i, at, :]
-        ])
-        from_far.append(send(far_out.at[i - 1], far_in.at[i - 1], {"tp": xor(tp, 2 * i)}))
-    from_core[0] = reduce_pair(0)
-
-    for c in range(CHUNKS):
+        from_core[i] = send(terms.at[pair * 2 + 1 - core], pair_in.at[i], {"tp": xor(tp, 1)})
+
+    def far_terms():
+        for i in far_pairs:
+            reduce_pair(i)
+
+    def far_sums():
+        for i in far_pairs:
+            from_core[i].wait_recv()
+            mine = xor(my_pair, i) * 2 + core
+
+            def keep_far(at, value, i=i):
+                far_out[i - 1, at, :] = value
+
+            add_rows(keep_far, [
+                lambda at, mine=mine: terms[mine, at, :], lambda at, i=i: pair_in[i, at, :]
+            ])
+            from_far.append(send(far_out.at[i - 1], far_in.at[i - 1], {"tp": xor(tp, 2 * i)}))
+
+    def near_terms():
+        reduce_pair(0)
+
+    def combine(c):
         wait_all(returned, c, plane - 1, p_recv.at[1, c])
         value = dot(mixing[...], returned[c].reshape(n_pos, cols)).astype(BF16)
         combined[c] = value.reshape(combined.shape[1:])
         z_copies(1, c, combined, final)
-    for c in range(CHUNKS):
+
+    def finish(c):
         wait_all(final, c, GROUPS - 1, z_recv.at[1, c])
         value = dot(choose_t[...], final[c].reshape(n_slots, cols))
         expert_out[:, c * cols : (c + 1) * cols] = value.astype(BF16)
 
-    from_core[0].wait_recv()
-    for copy in from_far:
-        copy.wait_recv()
-
-    def keep_out(at, value):
-        mixer_out[at, :] = value
-
-    add_rows(keep_out, [
-        lambda at: terms[tp, at, :], lambda at: pair_in[0, at, :]
-    ] + [lambda at, i=i: far_in[i, at, :] for i in range(pairs - 1)])
+    def mixer_sum():
+        from_core[0].wait_recv()
+        for copy in from_far:
+            copy.wait_recv()
+
+        def keep_out(at, value):
+            mixer_out[at, :] = value
+
+        add_rows(keep_out, [
+            lambda at: terms[tp, at, :], lambda at: pair_in[0, at, :]
+        ] + [lambda at, i=i: far_in[i, at, :] for i in range(pairs - 1)])
+
+    steps_by_name = locals()
+    for name, *args in order_of_steps:
+        steps_by_name[name](*args)
 
     for copy, when in singles:
         if when is None:
@@ -571,6 +610,17 @@
         wait_all(combined, c, GROUPS - 1, z_send.at[1, c])
         wait_all(sent, c, plane - 1, p_send.at[0, c])
         wait_all(result, c, plane - 1, p_send.at[1, c])
+
+
+def hand_out(mixed_in, expert_in, mixed_out, expert_out, sem):
+    copies = [
+        pltpu.make_async_copy(mixed_in, mixed_out, sem.at[0]),
+        pltpu.make_async_copy(expert_in, expert_out, sem.at[1]),
+    ]
+    for copy in copies:
+        copy.start()
+    for copy in copies:
+        copy.wait()
 
 
 def local(
@@ -594,7 +644,8 @@
     n_slots = GROUPS * slots
     n_pos = plane * block
     pairs = tp_count // 2
-    rounds = max(1, math.ceil(math.log2(ep_count))) + 1
+    rounds = len(state_strides(ep_count))
+    distances = sum(len(group) for group in state_strides(ep_count))
     coarse, fine = rope_tables(seg * ep_count)
 
     def buf(*shape, dtype=BF16):
@@ -602,7 +653,11 @@
 
     dma = pltpu.SemaphoreType.DMA
     scratch = [
-        buf(rows, width), buf(rows, width), buf(tp_count, rows, width),
+        buf(heads, seg, dtype=F32), buf(1, width, dtype=F32), buf(1, valw, dtype=F32),
+        buf(rows, width), buf(1, width, dtype=F32), buf(TOPK, rows, dtype=jnp.int32),
+        buf(1, rows, dtype=F32), buf(TOPK, rows, dtype=F32),
+        buf(seg // LOW, 2, KEY_DIM, dtype=F32), buf(2, LOW, KEY_DIM, dtype=F32),
+        buf(tp_count, rows, width), buf(tp_count, rows, width),
         buf(width, 2 * keyw + 2 * valw), buf(valw, width),
         buf(width, ff), buf(width, ff), buf(ff, width),
         buf(seg, 2 * keyw + 2 * valw),
@@ -615,28 +670,25 @@
         buf(CHUNKS, plane, block, cols), buf(CHUNKS, plane, block, cols),
         buf(CHUNKS, GROUPS, slots, cols), buf(CHUNKS, GROUPS, slots, cols),
         buf(GROUPS, slots, LANES), buf(GROUPS, slots, LANES),
-        buf(rounds, keyw, VALUE_DIM), buf(rounds, keyw, VALUE_DIM),
-        buf(rounds, 8, LANES, dtype=F32), buf(rounds, 8, LANES, dtype=F32),
-        buf(keyw, VALUE_DIM, dtype=F32),
+        buf(rounds, keyw, VALUE_DIM), buf(distances, keyw, VALUE_DIM),
+        buf(rounds, 8, LANES, dtype=F32), buf(distances, 8, LANES, dtype=F32),
+        buf(keyw, VALUE_DIM, dtype=F32), buf(8, LANES, dtype=F32),
         buf(seg, valw), buf(tp_count, rows, width), buf(pairs, rows, width),
         buf(max(1, pairs - 1), rows, width), buf(max(1, pairs - 1), rows, width),
-        dma((16,)), dma((32,)), dma((32,)),
+        dma((20,)), dma((32,)), dma((32,)),
         dma((2, CHUNKS)), dma((2, CHUNKS)), dma((2, CHUNKS)), dma((2, CHUNKS)),
     ]
     any_space = pl.BlockSpec(memory_space=pl.ANY)
     vmem = pl.BlockSpec(memory_space=pltpu.VMEM)
     shape = jax.ShapeDtypeStruct((rows, width), BF16)
-    return pl.pallas_call(
+    outs = pl.pallas_call(
         functools.partial(body, (ep_count, tp_count, cap)),
-        out_shape=(shape, shape),
-        in_specs=[
-            any_space, vmem, vmem, any_space, any_space, any_space, any_space, vmem, any_space,
-            any_space, vmem, vmem, vmem, vmem, any_space, any_space, any_space, vmem, vmem,
-        ],
+        out_shape=(buf(rows, width), buf(rows, width)),
+        in_specs=[any_space] * 19,
         out_specs=(vmem, vmem),
         scratch_shapes=scratch,
         compiler_params=pltpu.CompilerParams(
-            collective_id=0, has_side_effects=True, vmem_limit_bytes=67_000_000
+            collective_id=0, has_side_effects=True, vmem_limit_bytes=VMEM_LIMIT
         ),
     )(
         mixer_input, log_decay.T, mixer_gain[None, :], query_weight, key_weight, value_weight,
@@ -644,6 +696,14 @@
         routes.T, group_weight[None, :], pair_weight.T, expert_gate, expert_up, expert_down,
         jnp.asarray(coarse), jnp.asarray(fine),
     )
+    outs = [pltpu.with_memory_space_constraint(out, pltpu.VMEM) for out in outs]
+    return pl.pallas_call(
+        hand_out,
+        out_shape=(shape, shape),
+        in_specs=[vmem, vmem],
+        out_specs=(any_space, any_space),
+        scratch_shapes=[dma((2,))],
+    )(*outs)
 
 
 def solution(mesh):

time: 81.8 us -> 75.2 us (0.919)
  the two profiles are of different devices: /device:TPU:0 before, /device:TPU:24 now
where the time goes in v1:
time: 75.2 us; the launch traced here: 75 us
  Pallas kernels  74.2 us (99%)
  between operations  0.81 us (1%)
    pallas_call x1, Pallas kernels, local(): pl.pallas_call(functools.partial(body, (ep_count, tp_count, cap)), out_sh...  73.3 us

profile of v1, /device:TPU:24, one launch (start us, length us, event | category | flops | bytes accessed | tf_op | source)
XLA Modules:
  0.0 75.0 jit_solution(16760816078090901369)
XLA Ops:
  0.6 73.3 %shard_map.194 = (bf16[128,2048]{1,0:T(8,128)(2,1)S(1)}, bf16[128,2048]{1,0:T(8,128)(2,1)S(1)}) custom-call(bf16[128,2048]{1,0:T(8,128)(2,1)} %refs_0_.1, f32[2,512]{1,0:T(2,128)} %bitcast.9, f32[1,2048]{1,0:T(1,128)} %bitcast.7, bf16[2048,256]{1,0:T(8,128)(2,1)} %refs_3_.1, bf16[2048,256]{1,0:T(8,128)(2,1)} %refs_4_.1, bf16[2048,512]{1,0:T(8,128)(2,1)} %refs_5_.1, ...), custom_call_target="tpu_custom_call" | custom-call | tf_op jit(solution)/shard_map/pallas_call | solution.py:684
  73.9 1.0 %shard_map.195 = (bf16[128,2048]{1,0:T(8,128)(2,1)}, bf16[128,2048]{1,0:T(8,128)(2,1)}) custom-call(bf16[128,2048]{1,0:T(8,128)(2,1)S(1)} %get-tuple-element.4.mixed_in, bf16[128,2048]{1,0:T(8,128)(2,1)S(1)} %get-tuple-element.5.expert_in), custom_call_target="tpu_custom_call" | custom-call | tf_op jit(solution)/shard_map/pallas_call | solution.py:700

commit v2 on v1

--- a/solution.py
+++ b/solution.py
@@ -24,7 +24,7 @@
 BF16 = jnp.bfloat16
 
 ORDER = (
-    ("near_norm",), ("near_project",), ("spread_rows",), ("far_pass",), ("relay", 0), ("relay", 1), ("relay", 2), ("far_norm",), ("relay", 3), ("far_project",), ("states",), ("relay", 4), ("relay", 5), ("gate_up", 0), ("relay", 6), ("gate_up", 1), ("relay", 7), ("gate_up", 2), ("gate_up", 3), ("gate_up", 4), ("state_round", 0), ("down", 0), ("down", 1), ("down", 2), ("down", 3), ("down", 4), ("down", 5), ("down", 6), ("down", 7), ("queries",), ("combine", 0), ("state_round", 1), ("state_rest",), ("far_terms",), ("combine", 1), ("combine", 2), ("far_sums",), ("combine", 3), ("combine", 4), ("near_terms",), ("combine", 5), ("combine", 6), ("combine", 7), ("finish", 0), ("finish", 1), ("finish", 2), ("finish", 3), ("finish", 4), ("finish", 5), ("finish", 6), ("finish", 7), ("mixer_sum",),
+    ("near_norm",), ("spread_rows",), ("relay", 0), ("near_project",), ("relay", 1), ("far_pass",), ("relay_far", 0), ("relay_far", 1), ("relay", 2), ("relay_far", 2), ("far_norm",), ("relay", 3), ("relay_far", 3), ("far_project",), ("relay", 4), ("relay_far", 4), ("states",), ("relay", 5), ("relay_far", 5), ("gate_up", 0), ("relay", 6), ("relay_far", 6), ("relay", 7), ("relay_far", 7), ("state_send",), ("gate_up", 1), ("gate_up", 2), ("gate_up", 3), ("gate_up", 4), ("state_plane",), ("down", 0), ("down", 1), ("down", 2), ("down", 3), ("down", 4), ("state_hop", 0), ("down", 5), ("down", 6), ("down", 7), ("queries",), ("combine", 0), ("combine", 1), ("state_hop", 1), ("far_terms",), ("combine", 2), ("far_sums",), ("combine", 3), ("combine", 4), ("combine", 5), ("combine", 6), ("combine", 7), ("near_terms",), ("finish", 0), ("finish", 1), ("finish", 2), ("finish", 3), ("finish", 4), ("finish", 5), ("finish", 6), ("finish", 7), ("mixer_sum",),
 )
 
 
@@ -56,15 +56,6 @@
         np.stack([np.cos(coarse), np.sin(coarse)], axis=1).astype(np.float32),
         np.stack([np.cos(fine), np.sin(fine)], axis=0).astype(np.float32),
     )
-
-
-def state_strides(ep_count):
-    rounds = []
-    base = 1
-    while base < ep_count:
-        rounds.append([i * base for i in range(1, 4) if i * base < ep_count])
-        base *= 4
-    return rounds
 
 
 def norm_rows(source, gain, store, rows, step=32):
@@ -89,7 +80,7 @@
         choose_t, spread_t, mixing, normed,
         packed, relayed, sent, arrived, acc, hidden, result, returned, combined, final,
         meta_out, meta_in,
-        st_out, st_in, tot_out, tot_in, incoming, window_total,
+        st_out, st_in, tot_out, tot_in, incoming, whole, window_total,
         gated, terms, pair_in, far_out, far_in,
         load_sem, one_send, one_recv, z_send, z_recv, p_send, p_recv,
     ) = refs
@@ -121,8 +112,9 @@
     def place_peer(place):
         return at_flat(my_plane * plane + place)
 
-    rounds = state_strides(ep_count)
-    strides = [stride for group in rounds for stride in group]
+    inner = ep_count // GROUPS
+    inside = ep % inner
+    hops = [1 << b for b in range((GROUPS - 1).bit_length())]
 
     loads = {}
 
@@ -154,11 +146,6 @@
             barrier, inc=1, device_id=place_peer(xor(my_place, mask)), device_id_type=MESH
         )
         greeted += 1
-    for stride in sorted(set(strides)):
-        for other in ((ep + stride) % ep_count, (ep + ep_count - stride) % ep_count):
-            pl.semaphore_signal(barrier, inc=1, device_id=(other, tp), device_id_type=MESH)
-            greeted += 1
-
     singles = []
 
     def send(source, target, device, when=None):
@@ -258,9 +245,12 @@
                 device_id_type=MESH,
             ).start()
 
-    def p_copies(phase, c, source, target):
-        target[c, my_place] = source[c, my_place]
-        for mask in range(plane - 1, 0, -1):
+    masks = range(plane - 1, 0, -1)
+    across = [mask for mask in masks if mask % tp_count > 1]
+    aside = [mask for mask in masks if mask % tp_count <= 1]
+
+    def p_copies(phase, c, source, target, masks):
+        for mask in masks:
             other = xor(my_place, mask)
             pltpu.make_async_remote_copy(
                 src_ref=source.at[c, other],
@@ -364,7 +354,11 @@
         wait_all(relayed, c, GROUPS - 1, z_recv.at[0, c])
         value = dot(spread_t[...], relayed[c].reshape(n_slots, cols)).astype(BF16)
         sent[c] = value.reshape(sent.shape[1:])
-        p_copies(0, c, sent, arrived)
+        p_copies(0, c, sent, arrived, aside)
+        arrived[c, my_place] = sent[c, my_place]
+
+    def relay_far(c):
+        p_copies(0, c, sent, arrived, across)
 
     passed = []
 
@@ -387,18 +381,6 @@
     def rotated(first):
         x = proj[:, first : first + KEY_DIM].astype(F32)
         return x * cosine[...] + pltpu.roll(x, KEY_DIM // 2, 1) * sine[...]
-
-    prefix = {}
-
-    def state_send(r):
-        for stride in rounds[r]:
-            i = strides.index(stride)
-            device = {"ep": (ep + stride) % ep_count}
-            goes = ep + stride < ep_count
-            prefix[i] = (
-                send(tot_out.at[r], tot_in.at[i], device, goes),
-                send(st_out.at[r], st_in.at[i], device, goes),
-            )
 
     def states():
         for h in range(heads):
@@ -413,45 +395,75 @@
             )
             st_out[0, h * KEY_DIM : (h + 1) * KEY_DIM, :] = state.astype(BF16)
         tot_out[0] = jnp.broadcast_to(c_row[:, seg - 1 : seg], tot_out.shape[1:])
-        for i, stride in enumerate(strides):
-            @pl.when(ep < stride)
+        st_in[inside] = st_out[0]
+        tot_in[inside] = tot_out[0]
+        for b, hop in enumerate(hops):
+            @pl.when(my_plane < hop)
             def _():
-                st_in[i] = jnp.zeros(st_in.shape[1:], BF16)
-                tot_in[i] = jnp.zeros(tot_in.shape[1:], F32)
-        state_send(0)
-
-    def state_recv(i):
-        @pl.when(ep >= strides[i])
-        def _():
-            for copy in prefix[i]:
-                copy.wait_recv()
-
-    def state_round(r):
-        if r >= len(rounds):
-            return
-        for stride in rounds[r]:
-            i = strides.index(stride)
-            state_recv(i)
+                st_in[inner + b] = jnp.zeros(st_in.shape[1:], BF16)
+                tot_in[inner + b] = jnp.zeros(tot_in.shape[1:], F32)
+
+    arrivals = {}
+
+    def state_send():
+        arrivals[0] = []
+        for j in range(1, inner):
+            device = {"ep": my_plane * inner + (inside + j) % inner}
+            arrivals[0].append(send(tot_out.at[0], tot_in.at[inside], device))
+            arrivals[0].append(send(st_out.at[0], st_in.at[inside], device))
+
+    def plane_send(b):
+        if b < len(hops):
+            device = {"ep": (ep + hops[b] * inner) % ep_count}
+            goes = my_plane + hops[b] < GROUPS
+            st_out[b + 1] = whole[...].astype(BF16)
+            arrivals[b + 1] = [
+                send(tot_out.at[b + 1], tot_in.at[inner + b], device, goes),
+                send(st_out.at[b + 1], st_in.at[inner + b], device, goes),
+            ]
+
+    def state_plane():
+        for copy in arrivals[0]:
+            copy.wait_recv()
+        total = tot_in[0]
+        window = jnp.where(inside > 0, total, 0.0)
+        for h in range(heads):
+            at = slice(h * KEY_DIM, (h + 1) * KEY_DIM)
+            part = st_in[0, at, :].astype(F32)
+            whole[at, :] = part
+            incoming[at, :] = jnp.where(inside > 0, part, 0.0)
+        for i in range(1, inner):
             for h in range(heads):
                 at = slice(h * KEY_DIM, (h + 1) * KEY_DIM)
                 part = st_in[i, at, :].astype(F32)
-                if i > 0:
-                    scale = jnp.exp(window_total[h : h + 1, 0:1])
-                    part = incoming[at, :] + scale * part
-                incoming[at, :] = part
-            window_total[...] = tot_in[i] + (window_total[...] if i > 0 else 0.0)
-        if r + 1 < len(rounds):
-            for h in range(heads):
-                at = slice(h * KEY_DIM, (h + 1) * KEY_DIM)
-                scale = jnp.exp(tot_out[0, h : h + 1, 0:1])
-                whole = st_out[0, at, :].astype(F32) + scale * incoming[at, :]
-                st_out[r + 1, at, :] = whole.astype(BF16)
-            tot_out[r + 1] = tot_out[0] + window_total[...]
-            state_send(r + 1)
-
-    def state_rest():
-        for r in range(2, len(rounds)):
-            state_round(r)
+                scale = jnp.exp(tot_in[i, h : h + 1, 0:1])
+                whole[at, :] = part + scale * whole[at, :]
+                if i < inner - 1:
+                    joined = part + scale * incoming[at, :]
+                    incoming[at, :] = jnp.where(inside > i, joined, incoming[at, :])
+            total = total + tot_in[i]
+            window = jnp.where(inside > i, window + tot_in[i], window)
+        window_total[...] = window
+        tot_out[1] = total
+        plane_send(0)
+
+    def state_hop(b):
+        @pl.when(my_plane >= hops[b])
+        def _():
+            for copy in arrivals[b + 1]:
+                copy.wait_recv()
+
+        for h in range(heads):
+            at = slice(h * KEY_DIM, (h + 1) * KEY_DIM)
+            part = st_in[inner + b, at, :].astype(F32)
+            incoming[at, :] = incoming[at, :] + jnp.exp(window_total[h : h + 1, 0:1]) * part
+            if b + 1 < len(hops):
+                scale = jnp.exp(tot_out[b + 1, h : h + 1, 0:1])
+                whole[at, :] = whole[at, :] + scale * part
+        window_total[...] = window_total[...] + tot_in[inner + b]
+        if b + 1 < len(hops):
+            tot_out[b + 2] = tot_out[b + 1] + tot_in[inner + b]
+            plane_send(b + 1)
 
     def gate_up(c):
         if c == 0:
@@ -489,7 +501,8 @@
             value = dot(hidden[...], ed[:, wide]).astype(BF16)
             result[c, :, :, part] = value.reshape(plane, block, ftile)
 
-        p_copies(1, c, result, returned)
+        p_copies(1, c, result, returned, masks)
+        returned[c, my_place] = result[c, my_place]
 
     def queries():
         loads["wo"].wait()
@@ -644,8 +657,9 @@
     n_slots = GROUPS * slots
     n_pos = plane * block
     pairs = tp_count // 2
-    rounds = len(state_strides(ep_count))
-    distances = sum(len(group) for group in state_strides(ep_count))
+    hops = (GROUPS - 1).bit_length()
+    rounds = hops + 1
+    distances = ep_count // GROUPS + hops
     coarse, fine = rope_tables(seg * ep_count)
 
     def buf(*shape, dtype=BF16):
@@ -672,7 +686,7 @@
         buf(GROUPS, slots, LANES), buf(GROUPS, slots, LANES),
         buf(rounds, keyw, VALUE_DIM), buf(distances, keyw, VALUE_DIM),
         buf(rounds, 8, LANES, dtype=F32), buf(distances, 8, LANES, dtype=F32),
-        buf(keyw, VALUE_DIM, dtype=F32), buf(8, LANES, dtype=F32),
+        buf(keyw, VALUE_DIM, dtype=F32), buf(keyw, VALUE_DIM, dtype=F32), buf(8, LANES, dtype=F32),
         buf(seg, valw), buf(tp_count, rows, width), buf(pairs, rows, width),
         buf(max(1, pairs - 1), rows, width), buf(max(1, pairs - 1), rows, width),
         dma((20,)), dma((32,)), dma((32,)),

time: 75.2 us -> 71.2 us (0.947)
  the two profiles are of different devices: /device:TPU:24 before, /device:TPU:0 now
where the time goes in v2:
time: 71.2 us; the launch traced here: 71.1 us
  Pallas kernels  70.4 us (99%)
    pallas_call x1, Pallas kernels, local(): pl.pallas_call(functools.partial(body, (ep_count, tp_count, cap)), out_sh...  69.4 us

profile of v2, /device:TPU:0, one launch (start us, length us, event | category | flops | bytes accessed | tf_op | source)
XLA Modules:
  0.0 71.1 jit_solution(5779809662403250299)
XLA Ops:
  0.6 69.4 %shard_map.194 = (bf16[128,2048]{1,0:T(8,128)(2,1)S(1)}, bf16[128,2048]{1,0:T(8,128)(2,1)S(1)}) custom-call(bf16[128,2048]{1,0:T(8,128)(2,1)} %refs_0_.1, f32[2,512]{1,0:T(2,128)} %bitcast.9, f32[1,2048]{1,0:T(1,128)} %bitcast.7, bf16[2048,256]{1,0:T(8,128)(2,1)} %refs_3_.1, bf16[2048,256]{1,0:T(8,128)(2,1)} %refs_4_.1, bf16[2048,512]{1,0:T(8,128)(2,1)} %refs_5_.1, ...), custom_call_target="tpu_custom_call" | custom-call | tf_op jit(solution)/shard_map/pallas_call | solution.py:698
  70.1 1.0 %shard_map.195 = (bf16[128,2048]{1,0:T(8,128)(2,1)}, bf16[128,2048]{1,0:T(8,128)(2,1)}) custom-call(bf16[128,2048]{1,0:T(8,128)(2,1)S(1)} %get-tuple-element.4.mixed_in, bf16[128,2048]{1,0:T(8,128)(2,1)S(1)} %get-tuple-element.5.expert_in), custom_call_target="tpu_custom_call" | custom-call | tf_op jit(solution)/shard_map/pallas_call | solution.py:714

commit v3 on v2

--- a/solution.py
+++ b/solution.py
@@ -24,7 +24,17 @@
 BF16 = jnp.bfloat16
 
 ORDER = (
-    ("near_norm",), ("spread_rows",), ("relay", 0), ("near_project",), ("relay", 1), ("far_pass",), ("relay_far", 0), ("relay_far", 1), ("relay", 2), ("relay_far", 2), ("far_norm",), ("relay", 3), ("relay_far", 3), ("far_project",), ("relay", 4), ("relay_far", 4), ("states",), ("relay", 5), ("relay_far", 5), ("gate_up", 0), ("relay", 6), ("relay_far", 6), ("relay", 7), ("relay_far", 7), ("state_send",), ("gate_up", 1), ("gate_up", 2), ("gate_up", 3), ("gate_up", 4), ("state_plane",), ("down", 0), ("down", 1), ("down", 2), ("down", 3), ("down", 4), ("state_hop", 0), ("down", 5), ("down", 6), ("down", 7), ("queries",), ("combine", 0), ("combine", 1), ("state_hop", 1), ("far_terms",), ("combine", 2), ("far_sums",), ("combine", 3), ("combine", 4), ("combine", 5), ("combine", 6), ("combine", 7), ("near_terms",), ("finish", 0), ("finish", 1), ("finish", 2), ("finish", 3), ("finish", 4), ("finish", 5), ("finish", 6), ("finish", 7), ("mixer_sum",),
+    ("near_norm",), ("spread_rows",), ("relay", 0), ("near_project",), ("relay", 1),
+    ("far_pass",), ("relay_far", 0), ("relay_far", 1), ("relay", 2), ("relay_far", 2),
+    ("far_norm",), ("relay", 3), ("relay_far", 3), ("far_project",), ("relay", 4),
+    ("relay_far", 4), ("states",), ("relay", 5), ("relay_far", 5), ("gate_up", 0), ("relay", 6),
+    ("relay_far", 6), ("relay", 7), ("relay_far", 7), ("state_send",), ("gate_up", 1),
+    ("gate_up", 2), ("gate_up", 3), ("gate_up", 4), ("down", 0), ("state_plane",), ("down", 1),
+    ("down", 2), ("down", 3), ("down", 4), ("down", 5), ("state_hop", 0), ("down", 6),
+    ("down", 7), ("queries",), ("combine", 0), ("combine", 1), ("combine", 2), ("state_hop", 1),
+    ("far_terms",), ("combine", 3), ("combine", 4), ("far_sums",), ("combine", 5), ("combine", 6),
+    ("combine", 7), ("near_terms",), ("finish", 0), ("finish", 1), ("finish", 2), ("finish", 3),
+    ("finish", 4), ("finish", 5), ("finish", 6), ("finish", 7), ("mixer_sum",),
 )
 
 

time: 71.2 us -> 71.2 us (level)
  no operation moved by 1% of the time
where the time goes in v3:
time: 71.2 us; the launch traced here: 71 us
  Pallas kernels  70.4 us (99%)
    pallas_call x1, Pallas kernels, local(): pl.pallas_call(functools.partial(body, (ep_count, tp_count, cap)), out_sh...  69.4 us

profile of v3, /device:TPU:0, one launch (start us, length us, event | category | flops | bytes accessed | tf_op | source)
XLA Modules:
  0.0 71.0 jit_solution(10339938955456209026)
XLA Ops:
  0.6 69.4 %shard_map.194 = (bf16[128,2048]{1,0:T(8,128)(2,1)S(1)}, bf16[128,2048]{1,0:T(8,128)(2,1)S(1)}) custom-call(bf16[128,2048]{1,0:T(8,128)(2,1)} %refs_0_.1, f32[2,512]{1,0:T(2,128)} %bitcast.9, f32[1,2048]{1,0:T(1,128)} %bitcast.7, bf16[2048,256]{1,0:T(8,128)(2,1)} %refs_3_.1, bf16[2048,256]{1,0:T(8,128)(2,1)} %refs_4_.1, bf16[2048,512]{1,0:T(8,128)(2,1)} %refs_5_.1, ...), custom_call_target="tpu_custom_call" | custom-call | tf_op jit(solution)/shard_map/pallas_call | solution.py:708
  70.0 1.0 %shard_map.195 = (bf16[128,2048]{1,0:T(8,128)(2,1)}, bf16[128,2048]{1,0:T(8,128)(2,1)}) custom-call(bf16[128,2048]{1,0:T(8,128)(2,1)S(1)} %get-tuple-element.4.mixed_in, bf16[128,2048]{1,0:T(8,128)(2,1)S(1)} %get-tuple-element.5.expert_in), custom_call_target="tpu_custom_call" | custom-call | tf_op jit(solution)/shard_map/pallas_call | solution.py:724
